TPU v7x, 32 devices: a whole 2x2x4 slice. The times are simulated.
32 devices in a mesh: sp: 8 (over z, y), tp: 4 (over x, core).
Axes of the slice: x: 2, y: 2, z: 4, core: 2. Of those that a mesh axis runs over, the one named last changes fastest.
Arguments:
- stream: bfloat16 [4096, 2048], P('sp', 'tp'), may hold values from -6 to 6
- doc_ids: int32 [4096], P('sp'), may hold values from 0 to 3, never falling along the last dimension, each value on 1 to 2304 neighbouring positions
- norm_gain: float32 [2, 2048], replicated, may hold values from 0.1 to 1.9
- gate_proj: bfloat16 [2, 2048, 2048], P(None, 'sp', 'tp'), may hold values from -0.125 to 0.125
- input_gate: bfloat16 [2, 2048, 2048], P(None, 'sp', 'tp'), may hold values from -0.125 to 0.125
- value_proj: bfloat16 [2, 2048, 2048], P(None, 'sp', 'tp'), may hold values from -0.125 to 0.125
- taps: float32 [2, 3, 2048], P(None, None, 'tp'), may hold values from -3 to 3
- out_proj: bfloat16 [2, 2048, 2048], P(None, 'tp', 'sp'), may hold values from -0.125 to 0.125
Outputs:
- result: bfloat16 [4096, 2048], P('sp', 'tp')
Inputs may be any that keep to these rules, and one draw needn't show every extreme that they name: `doc_ids`: document numbers never fall along the sequence; each document holds 1 to 2304 positions.
All inputs are finite; a program needn't handle non-finite values.
Results may differ from a plain program's by a relative error of at most 0.03.
Values may be sent and summed in bfloat16 or wider, within the bound.
A program may use at most 64 MiB of HBM per device.

v0:
```python
import functools

import jax
import jax.numpy as jnp
from jax import lax
from jax.experimental import pallas as pl
from jax.experimental.pallas import tpu as pltpu
from jax.sharding import PartitionSpec as P

epsilon = 1e-06


def with_halo(value, sides, width):
    for axis, dim in sides:
        size, length = (lax.axis_size(axis), value.shape[dim])
        up = [(i, (i + 1) % size) for i in range(size - 1)]
        down = [(j, i) for i, j in up]
        last = lax.slice_in_dim(value, length - width, length, axis=dim)
        leading = lax.slice_in_dim(value, 0, width, axis=dim)
        before = lax.ppermute(last, axis, up)
        after = lax.ppermute(leading, axis, down)
        value = jnp.concatenate([before, value, after], axis=dim)
    return value


def per_device(stream, doc_ids, norm_gain, gate_proj, input_gate, value_proj, taps, out_proj):
    layers = gate_proj.shape[0]
    gathered_in = (
        lax.all_gather(gate_proj, "sp", axis=1, tiled=True),
        lax.all_gather(input_gate, "sp", axis=1, tiled=True),
        lax.all_gather(value_proj, "sp", axis=1, tiled=True),
    )
    gathered_out = lax.all_gather(out_proj, "sp", axis=2, tiled=True)
    current = stream
    for layer_index in range(layers):
        full_rows = lax.all_gather(current, "tp", axis=1, tiled=True)
        widened = full_rows.astype(jnp.float32)
        scale = lax.rsqrt(jnp.mean(widened * widened, axis=-1, keepdims=True) + epsilon)
        normed = (widened * scale * norm_gain[layer_index]).astype(jnp.bfloat16)
        gate_b = jnp.dot(normed, gathered_in[0][layer_index], preferred_element_type=jnp.float32)
        gate_c = jnp.dot(normed, gathered_in[1][layer_index], preferred_element_type=jnp.float32)
        values = jnp.dot(normed, gathered_in[2][layer_index], preferred_element_type=jnp.float32)
        gate_b = gate_b.astype(jnp.bfloat16)
        gate_c = gate_c.astype(jnp.bfloat16)
        values = values.astype(jnp.bfloat16)
        mixed_in = (gate_c.astype(jnp.float32) * values.astype(jnp.float32)).astype(jnp.bfloat16)
        padded, doc_padded = (
            with_halo(mixed_in, (("sp", 0),), 1),
            with_halo(doc_ids, (("sp", 0),), 1),
        )
        same_prev = (doc_padded[:-2] == doc_ids)[:, None]
        same_next = (doc_padded[2:] == doc_ids)[:, None]
        kernel_taps = taps[layer_index]
        convolved = (
            jnp.where(same_prev, kernel_taps[0] * padded[:-2].astype(jnp.float32), 0.0)
            + kernel_taps[1] * mixed_in.astype(jnp.float32)
            + jnp.where(same_next, kernel_taps[2] * padded[2:].astype(jnp.float32), 0.0)
        )
        gated = (gate_b.astype(jnp.float32) * convolved).astype(jnp.bfloat16)
        partials = jnp.dot(gated, gathered_out[layer_index], preferred_element_type=jnp.float32)
        summed = lax.psum_scatter(
            partials.astype(jnp.bfloat16), "tp", scatter_dimension=1, tiled=True
        ).astype(jnp.float32)
        current = (current.astype(jnp.float32) + summed).astype(jnp.bfloat16)
    return current


MESH = pl.DeviceIdType.MESH


def fused_kernel(S, T, L, stream_ref, docs_ref, gain_ref, gate_ref, input_ref, value_ref, taps_ref, outw_ref,
                 result_ref, win, wout, stage_in, stage_out, xfull, normed, cbuf, mpad, edge, halo, docall, docpad,
                 mprev, mnext, gated, dsrc, drcv, xsrc, xrcv, zsrc, zrcv, acc,
                 own_sem, w_send, y_send, w_recv, x_sem, agz_send, agx_send, agc_send, ag_recv,
                 d_send, d_recv, x_send, x_recv, z_send, z_recv, h_send, h_recv, doc_send, doc_recv):
    s = lax.axis_index("sp")
    t = lax.axis_index("tp")
    Z = S // 2
    z, y = s // 2, s % 2
    zh, zl = z // 2, z % 2
    x, c = t // 2, t % 2
    X = T // 2
    rows = stream_ref.shape[0]
    depth = gate_ref.shape[1]
    half = taps_ref.shape[2] // 2
    ow = outw_ref.shape[2]
    width = stream_ref.shape[1]
    per = width // ow
    units = 4 * L
    other_y = s + 1 - 2 * y
    sibling = t + 1 - 2 * c
    across = lax.rem(t + 2, T)
    mate = s + 2 - 4 * zl
    theirs = 1 - zl
    sources = (input_ref, value_ref, gate_ref)
    bf, f32 = jnp.bfloat16, jnp.float32
    pending = []

    barrier = pltpu.get_barrier_semaphore()

    def greet(sp_index, tp_index):
        pl.semaphore_signal(barrier, inc=1, device_id=(sp_index, tp_index), device_id_type=MESH)

    for k in range(1, S):
        greet(lax.rem(s + k, S), t)
    greet(s, sibling)
    greet(s, across)

    def remote(src, dst, send_sem, recv_sem, target):
        return pltpu.make_async_remote_copy(src_ref=src, dst_ref=dst, send_sem=send_sem, recv_sem=recv_sem,
                                            device_id=target, device_id_type=MESH)

    def go(copy_of):
        copy_of().start()
        pending.append(copy_of)

    def slot(u, shard):
        layer, part = u // 4, u % 4
        if part < 3:
            return win.at[layer * 3 + part, pl.ds(pl.multiple_of(shard * depth, depth), depth)]
        return wout.at[layer, shard]

    def stage(u):
        layer, part = u // 4, u % 4
        return stage_in.at[layer * 3 + part] if part < 3 else stage_out.at[layer]

    def own_copy(u, which):
        layer, part = u // 4, u % 4
        pick = pl.ds(pl.multiple_of((zl if which == 0 else theirs) * half, half), half)
        source = outw_ref.at[layer, pick, :] if part == 3 else sources[part].at[layer, :, pick]
        return pltpu.make_async_copy(source, slot(u, s) if which == 0 else stage(u), own_sem.at[u, which])

    def piece(layer, plane, owner, i):
        return xfull.at[layer, plane, owner, i]

    def x_copy(i):
        return pltpu.make_async_copy(stream_ref.at[:, i * ow:(i + 1) * ow], piece(0, zl, t, i), x_sem.at[i])

    for i in range(per):
        x_copy(i).start()
    for u in range(units):
        for which in range(2):
            own_copy(u, which).start()

    pl.semaphore_wait(barrier, S + 1)

    def z_copy(u, k):
        plane = lax.rem(z + k, Z)
        return remote(slot(u, s) if k % 2 == 0 else stage(u), slot(u, s), w_send.at[u, k], w_recv.at[u, s],
                      (2 * plane + y, t))

    def y_copy(u, plane):
        shard = 2 * plane + y
        return remote(slot(u, shard), slot(u, shard), y_send.at[u, plane], w_recv.at[u, shard], (other_y, t))

    def begin(u):
        if u >= units:
            return
        for which in range(2):
            own_copy(u, which).wait()
        for k in range(1, Z):
            go(lambda k=k: z_copy(u, k))
        go(lambda: y_copy(u, z))

    def arrived(u, shard):
        remote(slot(u, shard), slot(u, shard), y_send.at[u, z], w_recv.at[u, shard], (other_y, t)).wait_recv()

    def pump(u):
        if u >= units:
            return
        for k in range(1, Z):
            plane = lax.rem(z + k, Z)
            arrived(u, 2 * plane + y)
            go(lambda plane=plane: y_copy(u, plane))
        begin(u + 2)

    def need(u):
        for k in range(Z):
            plane = lax.rem(z + k, Z)
            arrived(u, 2 * plane + 1 - y)

    def agz(layer, i):
        return remote(piece(layer, zl, t, i), piece(layer, zl, t, i), agz_send.at[layer, i],
                      ag_recv.at[layer, zl, t, i], (mate, t))

    def agx(layer, plane, i):
        return remote(piece(layer, plane, t, i), piece(layer, plane, t, i), agx_send.at[layer, plane, i],
                      ag_recv.at[layer, plane, t, i], (s, across))

    def agc(layer, plane, owner, i):
        return remote(piece(layer, plane, owner, i), piece(layer, plane, owner, i),
                      agc_send.at[layer, plane, owner, i], ag_recv.at[layer, plane, owner, i], (s, sibling))

    def ag_wait(layer, plane, owner, i):
        remote(piece(layer, plane, owner, i), piece(layer, plane, owner, i), agz_send.at[layer, i],
               ag_recv.at[layer, plane, owner, i], (mate, t)).wait_recv()

    def ag_own(layer, i):
        go(lambda: agz(layer, i))
        go(lambda: agx(layer, zl, i))
        go(lambda: agc(layer, zl, t, i))

    def ag_from_z(layer, i):
        ag_wait(layer, theirs, t, i)
        go(lambda: agx(layer, theirs, i))
        go(lambda: agc(layer, theirs, t, i))

    def ag_from_x(layer, plane, i):
        ag_wait(layer, plane, across, i)
        go(lambda: agc(layer, plane, across, i))

    def ag_from_core(layer, plane):
        for i in range(per):
            ag_wait(layer, plane, sibling, i)
            ag_wait(layer, plane, lax.rem(sibling + 2, T), i)

    def doc_copy(k):
        return remote(docs_ref, docall.at[s], doc_send.at[k], doc_recv.at[s], (lax.rem(s + k, S), t))

    def group_block(b):
        return 2 * (2 * zh + b) + y

    def halo_copy(layer, b, side):
        target = lax.rem(group_block(b) + (1 if side == 0 else S - 1), S)
        core = 2 * (2 * (target // 4) + zl) + target % 2
        return remote(edge.at[layer, b, 1 - side], halo.at[layer, (target // 2) % 2, side],
                      h_send.at[layer, b, side], h_recv.at[layer, (target // 2) % 2, side], (core, t))

    def halo_wait(layer, b, side):
        remote(edge.at[layer, b, side], halo.at[layer, b, side], h_send.at[layer, b, side],
               h_recv.at[layer, b, side], (other_y, t)).wait_recv()

    for i in range(per):
        x_copy(i).wait()
        ag_own(0, i)
    for k in range(1, S):
        go(lambda k=k: doc_copy(k))
    begin(0)
    begin(1)

    small = rows // 8

    def norm(layer, plane):
        def step(r, carry):
            at = pl.ds(pl.multiple_of(r * small, small), small)
            total = jnp.zeros((small, 1), f32)
            for q in range(T):
                for i in range(per):
                    wide = xfull[layer, plane, q, i, at, :].astype(f32)
                    total = total + jnp.sum(wide * wide, axis=-1, keepdims=True)
            scale = lax.rsqrt(total / (width * T) + epsilon)
            for q in range(T):
                for i in range(per):
                    wide = xfull[layer, plane, q, i, at, :].astype(f32)
                    low = q * width + i * ow
                    gain = gain_ref[layer:layer + 1, low:low + ow]
                    normed[plane, at, low:low + ow] = (wide * scale * gain).astype(bf)
            return carry

        lax.fori_loop(0, rows // small, step, 0)

    def project(layer, part, plane):
        product = jnp.dot(normed[plane], win[layer * 3 + part], preferred_element_type=f32)
        return product.astype(bf)

    def both(layer, part, use):
        def step(e, carry):
            plane = lax.rem(zl + e, 2)
            use(plane, project(layer, part, plane))
            return carry

        lax.fori_loop(0, 2, step, 0)

    def keep_gate(plane, value):
        cbuf[plane] = value

    def mix(plane, value):
        mixed = (cbuf[plane].astype(f32) * value.astype(f32)).astype(bf)
        mpad[plane, 8:8 + rows, :] = mixed.astype(f32)

    def columns(block, row):
        line = docall[block, row:row + 1, :].astype(f32)
        return jnp.transpose(jnp.broadcast_to(line, (128, 128)))

    def masks():
        docall[s] = docs_ref[...]
        for k in range(1, S):
            remote(docs_ref, docall.at[lax.rem(s + k, S)], doc_send.at[k], doc_recv.at[lax.rem(s + k, S)],
                   (other_y, t)).wait_recv()
        lines = rows // 128
        for b in range(2):
            block = group_block(b)
            for j in range(lines):
                docpad[8 + 128 * j:136 + 128 * j, :] = columns(block, j)
            before = columns(lax.rem(block + S - 1, S), lines - 1)[120:128, :]
            after = columns(lax.rem(block + 1, S), 0)[0:8, :]
            docpad[0:8, :] = jnp.where(block > 0, before, -1.0)
            docpad[8 + rows:16 + rows, :] = jnp.where(block < S - 1, after, -1.0)
            here = docpad[8:8 + rows, :]
            mprev[b] = jnp.where(docpad[7:7 + rows, :] == here, 1.0, 0.0)
            mnext[b] = jnp.where(docpad[9:9 + rows, :] == here, 1.0, 0.0)

    def send_edges(layer):
        for b in range(2):
            edge[layer, b, 0] = mpad[b, 8:24, :].astype(bf)
            edge[layer, b, 1] = mpad[b, rows - 8:rows + 8, :].astype(bf)
        for b in range(2):
            for side in range(2):
                go(lambda b=b, side=side: halo_copy(layer, b, side))

    def convolve(layer):
        for b in range(2):
            for side in range(2):
                halo_wait(layer, b, side)
            mpad[b, 7:8, :] = halo[layer, b, 0, 15:16, :].astype(f32)
            mpad[b, 8 + rows:9 + rows, :] = halo[layer, b, 1, 0:1, :].astype(f32)
            for low in range(0, half, 128):
                lanes = slice(low, low + 128)
                tap = [jnp.where(zl == 0, taps_ref[j, layer:layer + 1, low:low + 128],
                                 taps_ref[j, layer:layer + 1, half + low:half + low + 128]) for j in range(3)]
                for r in range(0, rows, small):
                    before = tap[0] * mpad[b, r + 7:r + 7 + small, lanes]
                    middle = tap[1] * mpad[b, r + 8:r + 8 + small, lanes]
                    after = tap[2] * mpad[b, r + 9:r + 9 + small, lanes]
                    here = slice(r, r + small)
                    total = (jnp.where(mprev[b, here, :] > 0.5, before, 0.0) + middle
                             + jnp.where(mnext[b, here, :] > 0.5, after, 0.0))
                    gated[b, here, lanes] = (cbuf[b, here, lanes].astype(f32) * total).astype(bf)

    def owner_of(dx, dc):
        return lax.rem(x + dx, X) * 2 + lax.rem(c + dc, 2)

    def d_copy(layer, dx, i, tb):
        return remote(dsrc.at[layer, dx, i, tb], drcv.at[layer, dx, i, tb], d_send.at[layer, dx, i, tb],
                      d_recv.at[layer, dx, i, tb], (s, sibling))

    def xs_copy(layer, i, tb):
        return remote(xsrc.at[layer, i, tb], xrcv.at[layer, i, tb], x_send.at[layer, i, tb],
                      x_recv.at[layer, i, tb], (s, across))

    def zs_copy(layer, i):
        return remote(zsrc.at[layer, i], zrcv.at[layer, i], z_send.at[layer, i], z_recv.at[layer, i], (mate, t))

    def sweep(use):
        def step(e, carry):
            use(e // 2, e % 2)
            return carry

        lax.fori_loop(0, 2 * per, step, 0)

    def partial(layer, dx, dc, i, tb):
        shard = owner_of(dx, dc) * per + i
        return jnp.dot(gated[lax.rem(theirs + tb, 2)], wout[layer, shard], preferred_element_type=f32)

    def hand_over(layer, dx):
        def use(i, tb):
            dsrc[layer, dx, i, tb] = partial(layer, dx, 1, i, tb).astype(bf)
            d_copy(layer, dx, i, tb).start()

        sweep(use)

    def send_across(layer):
        def use(i, tb):
            part = partial(layer, 1, 0, i, tb)
            d_copy(layer, 1, i, tb).wait_recv()
            xsrc[layer, i, tb] = (part + drcv[layer, 1, i, tb].astype(f32)).astype(bf)
            xs_copy(layer, i, tb).start()

        sweep(use)

    def hold(layer):
        def use(i, tb):
            part = partial(layer, 0, 0, i, tb)
            d_copy(layer, 0, i, tb).wait_recv()
            acc[i, tb] = part + drcv[layer, 0, i, tb].astype(f32)

        sweep(use)

    def to_mate(layer, i):
        xs_copy(layer, i, 0).wait_recv()
        zsrc[layer, i] = (acc[i, 0] + xrcv[layer, i, 0].astype(f32)).astype(bf)
        go(lambda: zs_copy(layer, i))

    def finish(layer, i):
        xs_copy(layer, i, 1).wait_recv()
        zs_copy(layer, i).wait_recv()
        total = acc[i, 1] + xrcv[layer, i, 1].astype(f32) + zrcv[layer, i].astype(f32)
        fresh = (xfull[layer, zl, t, i].astype(f32) + total).astype(bf)
        if layer + 1 < L:
            xfull[layer + 1, zl, t, i] = fresh
        else:
            result_ref[:, i * ow:(i + 1) * ow] = fresh

    pump(0)
    for layer in range(L):
        base = 4 * layer
        for i in range(per):
            ag_from_z(layer, i)
        if layer == 0:
            masks()
        for i in range(per):
            ag_from_x(layer, zl, i)
        for i in range(per):
            ag_from_x(layer, theirs, i)
        pump(base + 1)
        ag_from_core(layer, zl)
        norm(layer, zl)
        ag_from_core(layer, theirs)
        norm(layer, theirs)
        need(base)
        both(layer, 0, keep_gate)
        pump(base + 2)
        need(base + 1)
        both(layer, 1, mix)
        send_edges(layer)
        need(base + 2)
        both(layer, 2, keep_gate)
        convolve(layer)
        pump(base + 3)
        need(base + 3)
        hand_over(layer, 1)
        send_across(layer)
        hand_over(layer, 0)
        hold(layer)
        pump(base + 4)
        for i in range(per):
            to_mate(layer, i)
        for i in range(per):
            finish(layer, i)
            if layer + 1 < L:
                ag_own(layer + 1, i)

    for copy_of in pending:
        copy_of().wait_send()
    for layer in range(L):
        def drain(i, tb):
            for dx in range(2):
                d_copy(layer, dx, i, tb).wait_send()
            xs_copy(layer, i, tb).wait_send()

        sweep(drain)


def fused(S, T, stream, doc_ids, norm_gain, gate_proj, input_gate, value_proj, taps, out_proj):
    rows, width = stream.shape
    L, depth, cols = gate_proj.shape
    ow = out_proj.shape[2]
    per, half = width // ow, cols // 2
    bf, f32, i32 = jnp.bfloat16, jnp.float32, jnp.int32
    docs = doc_ids.reshape(rows // 128, 128)
    vmem, hbm = pl.BlockSpec(memory_space=pltpu.VMEM), pl.BlockSpec(memory_space=pl.ANY)
    dma = pltpu.SemaphoreType.DMA
    scratch = [
        pltpu.VMEM((3 * L, S * depth, half), bf),
        pltpu.VMEM((L, S, half, ow), bf),
        pltpu.VMEM((3 * L, depth, half), bf),
        pltpu.VMEM((L, half, ow), bf),
        pltpu.VMEM((L, 2, T, per, rows, ow), bf),
        pltpu.VMEM((2, rows, T * width), bf),
        pltpu.VMEM((2, rows, half), bf),
        pltpu.VMEM((2, rows + 16, half), f32),
        pltpu.VMEM((L, 2, 2, 16, half), bf),
        pltpu.VMEM((L, 2, 2, 16, half), bf),
        pltpu.VMEM((S, rows // 128, 128), i32),
        pltpu.VMEM((rows + 16, 128), f32),
        pltpu.VMEM((2, rows, 128), f32),
        pltpu.VMEM((2, rows, 128), f32),
        pltpu.VMEM((2, rows, half), bf),
        pltpu.VMEM((L, 2, per, 2, rows, ow), bf),
        pltpu.VMEM((L, 2, per, 2, rows, ow), bf),
        pltpu.VMEM((L, per, 2, rows, ow), bf),
        pltpu.VMEM((L, per, 2, rows, ow), bf),
        pltpu.VMEM((L, per, rows, ow), bf),
        pltpu.VMEM((L, per, rows, ow), bf),
        pltpu.VMEM((per, 2, rows, ow), f32),
        dma((4 * L, 2)),
        dma((4 * L, S // 2)),
        dma((4 * L, S // 2)),
        dma((4 * L, S)),
        dma((per,)),
        dma((L, per)),
        dma((L, 2, per)),
        dma((L, 2, T, per)),
        dma((L, 2, T, per)),
        dma((L, 2, per, 2)),
        dma((L, 2, per, 2)),
        dma((L, per, 2)),
        dma((L, per, 2)),
        dma((L, per)),
        dma((L, per)),
        dma((L, 2, 2)),
        dma((L, 2, 2)),
        dma((S,)),
        dma((S,)),
    ]
    return pl.pallas_call(
        functools.partial(fused_kernel, S, T, L),
        out_shape=jax.ShapeDtypeStruct((rows, width), bf),
        in_specs=[hbm, vmem, vmem, hbm, hbm, hbm, vmem, hbm],
        out_specs=vmem,
        scratch_shapes=scratch,
        compiler_params=pltpu.CompilerParams(
            collective_id=0, has_side_effects=True, vmem_limit_bytes=60 * 1024 * 1024),
    )(stream, docs, norm_gain, gate_proj, input_gate, value_proj, jnp.transpose(taps, (1, 0, 2)), out_proj)


def solution(mesh):
    sp, tp = mesh.shape["sp"], mesh.shape["tp"]

    def body(*arrays):
        (rows, width), cols, out_width = arrays[0].shape, arrays[3].shape[2], arrays[7].shape[2]
        aligned = out_width % 128 == 0 and cols % 256 == 0 and rows % 128 == 0 and width % out_width == 0
        if aligned and sp % 4 == 0 and tp == 4:
            return fused(sp, tp, *arrays)
        return per_device(*arrays)

    in_specs = (
        P("sp", "tp"),
        P("sp"),
        P(),
        P(None, "sp", "tp"),
        P(None, "sp", "tp"),
        P(None, "sp", "tp"),
        P(None, None, "tp"),
        P(None, "tp", "sp"),
    )
    out_specs = P("sp", "tp")
    return jax.shard_map(
        body, mesh=mesh, in_specs=in_specs, out_specs=out_specs, check_vma=False
    )
```

profile of v0, /device:TPU:5, one launch (start us, length us, event | category | flops | bytes accessed | tf_op | source)
XLA Modules:
  0.0 193.8 jit_solution(12327250103484406358)
XLA Ops:
  0.0 191.9 %shard_map.82 = bf16[512,512]{1,0:T(8,128)(2,1)} custom-call(bf16[512,512]{1,0:T(8,128)(2,1)} %stream_ref.1, s32[4,128]{1,0:T(4,128)} %bitcast.3, f32[2,2048]{1,0:T(2,128)} %gain_ref.1, bf16[2,256,512]{2,1,0:T(8,128)(2,1)} %gate_ref.1, bf16[2,256,512]{2,1,0:T(8,128)(2,1)} %input_ref.1, bf16[2,256,512]{2,1,0:T(8,128)(2,1)} %value_ref.1, ...), custom_call_target="tpu_custom_call" | custom-call | tf_op jit(solution)/shard_map/pallas_call | solution.py:496
  191.9 1.9 copy.10
where the time goes:
time: 197 us; the launch traced here: 194 us
  Pallas kernels  192 us (97%)
    pallas_call x1, Pallas kernels, fused(): pl.pallas_call(functools.partial(fused_kernel, S, T, L), out_shape=jax.Sh...  192 us

commit v1 on v0

--- a/solution.py
+++ b/solution.py
@@ -72,7 +72,7 @@
                  result_ref, win, wout, stage_in, stage_out, xfull, normed, cbuf, mpad, edge, halo, docall, docpad,
                  mprev, mnext, gated, dsrc, drcv, xsrc, xrcv, zsrc, zrcv, acc,
                  own_sem, w_send, y_send, w_recv, x_sem, agz_send, agx_send, agc_send, ag_recv,
-                 d_send, d_recv, x_send, x_recv, z_send, z_recv, h_send, h_recv, doc_send, doc_recv):
+                 d_send, d_recv, x_send, x_recv, z_send, z_recv, h_send, h_recv, doc_send, doc_recv, pace):
     s = lax.axis_index("sp")
     t = lax.axis_index("tp")
     Z = S // 2
@@ -110,9 +110,12 @@
         return pltpu.make_async_remote_copy(src_ref=src, dst_ref=dst, send_sem=send_sem, recv_sem=recv_sem,
                                             device_id=target, device_id_type=MESH)
 
-    def go(copy_of):
-        copy_of().start()
-        pending.append(copy_of)
+    def go(copy_of, cond=None):
+        if cond is None:
+            copy_of().start()
+        else:
+            pl.when(cond)(lambda: copy_of().start())
+        pending.append((copy_of, cond))
 
     def slot(u, shard):
         layer, part = u // 4, u % 4
@@ -153,26 +156,25 @@
         shard = 2 * plane + y
         return remote(slot(u, shard), slot(u, shard), y_send.at[u, plane], w_recv.at[u, shard], (other_y, t))
 
+    def own_y(u):
+        go(lambda: y_copy(u, z))
+
     def begin(u):
-        if u >= units:
-            return
-        for which in range(2):
-            own_copy(u, which).wait()
         for k in range(1, Z):
             go(lambda k=k: z_copy(u, k))
-        go(lambda: y_copy(u, z))
 
     def arrived(u, shard):
         remote(slot(u, shard), slot(u, shard), y_send.at[u, z], w_recv.at[u, shard], (other_y, t)).wait_recv()
 
-    def pump(u):
-        if u >= units:
-            return
-        for k in range(1, Z):
-            plane = lax.rem(z + k, Z)
+    def pump(u, low=1, high=Z):
+        for k in range(low, high):
+            plane = lax.rem(z + Z + (2 * zl - 1) * k, Z)
             arrived(u, 2 * plane + y)
             go(lambda plane=plane: y_copy(u, plane))
-        begin(u + 2)
+
+    def meet(u):
+        pl.semaphore_signal(pace.at[u], inc=1, device_id=(s, sibling), device_id_type=MESH)
+        pl.semaphore_wait(pace.at[u], 1)
 
     def need(u):
         for k in range(Z):
@@ -230,11 +232,16 @@
         remote(edge.at[layer, b, side], halo.at[layer, b, side], h_send.at[layer, b, side],
                h_recv.at[layer, b, side], (other_y, t)).wait_recv()
 
+    for k in range(1, S):
+        go(lambda k=k: doc_copy(k))
     for i in range(per):
         x_copy(i).wait()
         ag_own(0, i)
-    for k in range(1, S):
-        go(lambda k=k: doc_copy(k))
+    for u in range(units):
+        for which in range(2):
+            own_copy(u, which).wait()
+    for u in range(5):
+        own_y(u)
     begin(0)
     begin(1)
 
@@ -260,23 +267,12 @@
         lax.fori_loop(0, rows // small, step, 0)
 
     def project(layer, part, plane):
-        product = jnp.dot(normed[plane], win[layer * 3 + part], preferred_element_type=f32)
-        return product.astype(bf)
-
-    def both(layer, part, use):
-        def step(e, carry):
-            plane = lax.rem(zl + e, 2)
-            use(plane, project(layer, part, plane))
-            return carry
-
-        lax.fori_loop(0, 2, step, 0)
-
-    def keep_gate(plane, value):
-        cbuf[plane] = value
-
-    def mix(plane, value):
-        mixed = (cbuf[plane].astype(f32) * value.astype(f32)).astype(bf)
-        mpad[plane, 8:8 + rows, :] = mixed.astype(f32)
+        product = jnp.dot(normed[plane], win[layer * 3 + part], preferred_element_type=f32).astype(bf)
+        if part == 1:
+            mixed = (cbuf[plane].astype(f32) * product.astype(f32)).astype(bf)
+            mpad[plane, 8:8 + rows, :] = mixed.astype(f32)
+        else:
+            cbuf[plane] = product
 
     def columns(block, row):
         line = docall[block, row:row + 1, :].astype(f32)
@@ -300,20 +296,36 @@
             mprev[b] = jnp.where(docpad[7:7 + rows, :] == here, 1.0, 0.0)
             mnext[b] = jnp.where(docpad[9:9 + rows, :] == here, 1.0, 0.0)
 
-    def send_edges(layer):
-        for b in range(2):
-            edge[layer, b, 0] = mpad[b, 8:24, :].astype(bf)
-            edge[layer, b, 1] = mpad[b, rows - 8:rows + 8, :].astype(bf)
-        for b in range(2):
-            for side in range(2):
-                go(lambda b=b, side=side: halo_copy(layer, b, side))
+    def send_edges(layer, b):
+        edge[layer, b, 0] = mpad[b, 8:24, :].astype(bf)
+        edge[layer, b, 1] = mpad[b, rows - 8:rows + 8, :].astype(bf)
+        block = group_block(b)
+        go(lambda: halo_copy(layer, b, 0), block < S - 1)
+        go(lambda: halo_copy(layer, b, 1), block > 0)
 
     def convolve(layer):
         for b in range(2):
-            for side in range(2):
-                halo_wait(layer, b, side)
-            mpad[b, 7:8, :] = halo[layer, b, 0, 15:16, :].astype(f32)
-            mpad[b, 8 + rows:9 + rows, :] = halo[layer, b, 1, 0:1, :].astype(f32)
+            block = group_block(b)
+            empty = jnp.zeros((1, half), f32)
+
+            @pl.when(block > 0)
+            def _():
+                halo_wait(layer, b, 0)
+                mpad[b, 7:8, :] = halo[layer, b, 0, 15:16, :].astype(f32)
+
+            @pl.when(block == 0)
+            def _():
+                mpad[b, 7:8, :] = empty
+
+            @pl.when(block < S - 1)
+            def _():
+                halo_wait(layer, b, 1)
+                mpad[b, 8 + rows:9 + rows, :] = halo[layer, b, 1, 0:1, :].astype(f32)
+
+            @pl.when(block == S - 1)
+            def _():
+                mpad[b, 8 + rows:9 + rows, :] = empty
+
             for low in range(0, half, 128):
                 lanes = slice(low, low + 128)
                 tap = [jnp.where(zl == 0, taps_ref[j, layer:layer + 1, low:low + 128],
@@ -343,7 +355,7 @@
 
     def sweep(use):
         def step(e, carry):
-            use(e // 2, e % 2)
+            use(e % per, e // per)
             return carry
 
         lax.fori_loop(0, 2 * per, step, 0)
@@ -391,47 +403,90 @@
         else:
             result_ref[:, i * ow:(i + 1) * ow] = fresh
 
-    pump(0)
     for layer in range(L):
         base = 4 * layer
-        for i in range(per):
-            ag_from_z(layer, i)
+        last = layer == L - 1
         if layer == 0:
+            pump(0, 1, Z - 1)
+            for i in range(per):
+                ag_from_x(layer, zl, i)
+            for i in range(per):
+                ag_from_z(layer, i)
+            pump(0, Z - 1, Z)
+            meet(0)
+            begin(2)
             masks()
-        for i in range(per):
-            ag_from_x(layer, zl, i)
+            pump(1, 1, Z - 1)
+            pump(1, Z - 1, Z)
+            meet(1)
+            begin(3)
+        else:
+            pump(base + 2)
+            for i in range(per):
+                ag_from_z(layer, i)
+                ag_from_x(layer, zl, i)
+        ag_from_core(layer, zl)
+        norm(layer, zl)
+        need(base)
+        project(layer, 0, zl)
+        if layer == 0:
+            pump(2, 1, Z - 1)
+        need(base + 1)
+        project(layer, 1, zl)
+        send_edges(layer, zl)
+        if layer == 0:
+            pump(2, Z - 1, Z)
+        else:
+            pump(base + 3)
+            need(base + 2)
+            project(layer, 2, zl)
         for i in range(per):
             ag_from_x(layer, theirs, i)
-        pump(base + 1)
-        ag_from_core(layer, zl)
-        norm(layer, zl)
         ag_from_core(layer, theirs)
         norm(layer, theirs)
-        need(base)
-        both(layer, 0, keep_gate)
-        pump(base + 2)
-        need(base + 1)
-        both(layer, 1, mix)
-        send_edges(layer)
-        need(base + 2)
-        both(layer, 2, keep_gate)
+        project(layer, 0, theirs)
+        project(layer, 1, theirs)
+        send_edges(layer, theirs)
+        if not last:
+            begin(base + 4)
+        if layer == 0:
+            pump(3, 1, Z - 1)
+            need(base + 2)
+            project(layer, 2, zl)
+        project(layer, 2, theirs)
+        if layer == 0:
+            pump(3, Z - 1, Z)
+        if not last:
+            meet(base + 3)
+            begin(base + 5)
         convolve(layer)
-        pump(base + 3)
         need(base + 3)
+        if not last:
+            for u in range(base + 5, base + 8):
+                own_y(u)
         hand_over(layer, 1)
         send_across(layer)
         hand_over(layer, 0)
         hold(layer)
-        pump(base + 4)
+        if not last:
+            pump(base + 4)
         for i in range(per):
             to_mate(layer, i)
+        if not last:
+            begin(base + 6)
+            pump(base + 5)
         for i in range(per):
             finish(layer, i)
-            if layer + 1 < L:
+            if not last:
                 ag_own(layer + 1, i)
-
-    for copy_of in pending:
-        copy_of().wait_send()
+        if not last:
+            begin(base + 7)
+
+    for copy_of, cond in pending:
+        if cond is None:
+            copy_of().wait_send()
+        else:
+            pl.when(cond)(lambda copy_of=copy_of: copy_of().wait_send())
     for layer in range(L):
         def drain(i, tb):
             for dx in range(2):
@@ -492,6 +547,7 @@
         dma((L, 2, 2)),
         dma((S,)),
         dma((S,)),
+        pltpu.SemaphoreType.REGULAR((4 * L,)),
     ]
     return pl.pallas_call(
         functools.partial(fused_kernel, S, T, L),

time: 197 us -> 168 us (0.85); the launches traced: 194 us -> 167 us
  Pallas kernels: 192 us -> 165 us
    pallas_call x1, Pallas kernels: 192 us -> 165 us  [fused(): pl.pallas_call(functools.partial(fused_kernel, S, T, L), out_shape=jax.Sh...]
where the time goes in v1:
time: 168 us; the launch traced here: 167 us
  Pallas kernels  165 us (98%)
  local copies, waits for them, and re-layouts  1.87 us (1%)
    pallas_call x1, Pallas kernels, fused(): pl.pallas_call(functools.partial(fused_kernel, S, T, L), out_shape=jax.Sh...  165 us

profile of v1, /device:TPU:5, one launch (start us, length us, event | category | flops | bytes accessed | tf_op | source)
XLA Modules:
  0.0 167.3 jit_solution(8854769614908684425)
XLA Ops:
  0.0 165.5 %shard_map.82 = bf16[512,512]{1,0:T(8,128)(2,1)} custom-call(bf16[512,512]{1,0:T(8,128)(2,1)} %stream_ref.1, s32[4,128]{1,0:T(4,128)} %bitcast.3, f32[2,2048]{1,0:T(2,128)} %gain_ref.1, bf16[2,256,512]{2,1,0:T(8,128)(2,1)} %gate_ref.1, bf16[2,256,512]{2,1,0:T(8,128)(2,1)} %input_ref.1, bf16[2,256,512]{2,1,0:T(8,128)(2,1)} %value_ref.1, ...), custom_call_target="tpu_custom_call" | custom-call | tf_op jit(solution)/shard_map/pallas_call | solution.py:552
  165.5 1.9 %copy.10 = bf16[512,512]{1,0:T(8,128)(2,1)} copy(bf16[512,512]{1,0:T(8,128)(2,1)} %shard_map.82) | data formatting | bytes 1048576

commit v2 on v1

--- a/solution.py
+++ b/solution.py
@@ -70,9 +70,10 @@
 
 def fused_kernel(S, T, L, stream_ref, docs_ref, gain_ref, gate_ref, input_ref, value_ref, taps_ref, outw_ref,
                  result_ref, win, wout, stage_in, stage_out, xfull, normed, cbuf, mpad, edge, halo, docall, docpad,
-                 mprev, mnext, gated, dsrc, drcv, xsrc, xrcv, zsrc, zrcv, acc,
+                 mprev, mnext, gated, dsrc, drcv, xsrc, xrcv, zsrc, zrcv, acc, zqsrc, zqrcv, xqsrc, xqrcv, accq,
                  own_sem, w_send, y_send, w_recv, x_sem, agz_send, agx_send, agc_send, ag_recv,
-                 d_send, d_recv, x_send, x_recv, z_send, z_recv, h_send, h_recv, doc_send, doc_recv, pace):
+                 d_send, d_recv, x_send, x_recv, z_send, z_recv, h_send, h_recv, doc_send, doc_recv, pace,
+                 zq_send, zq_recv, xq_send, xq_recv):
     s = lax.axis_index("sp")
     t = lax.axis_index("tp")
     Z = S // 2
@@ -240,7 +241,7 @@
     for u in range(units):
         for which in range(2):
             own_copy(u, which).wait()
-    for u in range(5):
+    for u in range(4):
         own_y(u)
     begin(0)
     begin(1)
@@ -388,6 +389,50 @@
 
         sweep(use)
 
+    def joined(layer, dx, i, tb):
+        part = partial(layer, dx, 0, i, tb)
+        d_copy(layer, dx, i, tb).wait_recv()
+        return part + drcv[layer, dx, i, tb].astype(f32)
+
+    tail = per - 1
+
+    def zq_copy(dx):
+        return remote(zqsrc.at[dx], zqrcv.at[dx], zq_send.at[dx], zq_recv.at[dx], (mate, t))
+
+    def xq_copy():
+        return remote(xqsrc, xqrcv, xq_send, xq_recv, (s, across))
+
+    def to_mate_first(layer, dx):
+        zqsrc[dx] = joined(layer, dx, tail, 0).astype(bf)
+        go(lambda: zq_copy(dx))
+
+    def send_both(layer):
+        to_mate_first(layer, 1)
+        for tb in range(2):
+            for i in range(tail):
+                xsrc[layer, i, tb] = joined(layer, 1, i, tb).astype(bf)
+                go(lambda i=i, tb=tb: xs_copy(layer, i, tb))
+        accq[...] = joined(layer, 1, tail, 1)
+
+    def hold_both(layer):
+        to_mate_first(layer, 0)
+        for tb in range(2):
+            for i in range(tail):
+                acc[i, tb] = joined(layer, 0, i, tb)
+        acc[tail, 1] = joined(layer, 0, tail, 1)
+
+    def cross_sum():
+        zq_copy(1).wait_recv()
+        xqsrc[...] = (accq[...] + zqrcv[1].astype(f32)).astype(bf)
+        go(xq_copy)
+
+    def finish_crossed(layer):
+        zq_copy(0).wait_recv()
+        xq_copy().wait_recv()
+        total = acc[tail, 1] + zqrcv[0].astype(f32) + xqrcv[...].astype(f32)
+        fresh = (xfull[layer, zl, t, tail].astype(f32) + total).astype(bf)
+        result_ref[:, tail * ow:(tail + 1) * ow] = fresh
+
     def to_mate(layer, i):
         xs_copy(layer, i, 0).wait_recv()
         zsrc[layer, i] = (acc[i, 0] + xrcv[layer, i, 0].astype(f32)).astype(bf)
@@ -408,25 +453,27 @@
         last = layer == L - 1
         if layer == 0:
             pump(0, 1, Z - 1)
+            meet(0)
+            begin(2)
             for i in range(per):
                 ag_from_x(layer, zl, i)
             for i in range(per):
                 ag_from_z(layer, i)
             pump(0, Z - 1, Z)
-            meet(0)
-            begin(2)
             masks()
-            pump(1, 1, Z - 1)
-            pump(1, Z - 1, Z)
+            pump(1)
             meet(1)
             begin(3)
         else:
             pump(base + 2)
+            ag_from_z(layer, 0)
             for i in range(per):
-                ag_from_z(layer, i)
                 ag_from_x(layer, zl, i)
         ag_from_core(layer, zl)
         norm(layer, zl)
+        if layer > 0:
+            for i in range(1, per):
+                ag_from_z(layer, i)
         need(base)
         project(layer, 0, zl)
         if layer == 0:
@@ -438,8 +485,6 @@
             pump(2, Z - 1, Z)
         else:
             pump(base + 3)
-            need(base + 2)
-            project(layer, 2, zl)
         for i in range(per):
             ag_from_x(layer, theirs, i)
         ag_from_core(layer, theirs)
@@ -447,39 +492,47 @@
         project(layer, 0, theirs)
         project(layer, 1, theirs)
         send_edges(layer, theirs)
+        if layer == 0:
+            pump(3)
         if not last:
             begin(base + 4)
-        if layer == 0:
-            pump(3, 1, Z - 1)
-            need(base + 2)
-            project(layer, 2, zl)
+        need(base + 2)
+        project(layer, 2, zl)
         project(layer, 2, theirs)
-        if layer == 0:
-            pump(3, Z - 1, Z)
         if not last:
             meet(base + 3)
             begin(base + 5)
         convolve(layer)
         need(base + 3)
         if not last:
-            for u in range(base + 5, base + 8):
+            begin(base + 6)
+            for u in range(base + 4, base + 8):
                 own_y(u)
         hand_over(layer, 1)
-        send_across(layer)
+        if last:
+            send_both(layer)
+        else:
+            send_across(layer)
         hand_over(layer, 0)
-        hold(layer)
+        if last:
+            hold_both(layer)
+        else:
+            hold(layer)
         if not last:
             pump(base + 4)
-        for i in range(per):
+        for i in range(per - 1 if last else per):
             to_mate(layer, i)
-        if not last:
-            begin(base + 6)
+        if last:
+            cross_sum()
+        else:
             pump(base + 5)
-        for i in range(per):
+        for i in range(per - 1 if last else per):
             finish(layer, i)
             if not last:
                 ag_own(layer + 1, i)
-        if not last:
+        if last:
+            finish_crossed(layer)
+        else:
             begin(base + 7)
 
     for copy_of, cond in pending:
@@ -491,7 +544,8 @@
         def drain(i, tb):
             for dx in range(2):
                 d_copy(layer, dx, i, tb).wait_send()
-            xs_copy(layer, i, tb).wait_send()
+            if layer + 1 < L:
+                xs_copy(layer, i, tb).wait_send()
 
         sweep(drain)
 
@@ -528,6 +582,11 @@
         pltpu.VMEM((L, per, rows, ow), bf),
         pltpu.VMEM((L, per, rows, ow), bf),
         pltpu.VMEM((per, 2, rows, ow), f32),
+        pltpu.VMEM((2, rows, ow), bf),
+        pltpu.VMEM((2, rows, ow), bf),
+        pltpu.VMEM((rows, ow), bf),
+        pltpu.VMEM((rows, ow), bf),
+        pltpu.VMEM((rows, ow), f32),
         dma((4 * L, 2)),
         dma((4 * L, S // 2)),
         dma((4 * L, S // 2)),
@@ -548,6 +607,10 @@
         dma((S,)),
         dma((S,)),
         pltpu.SemaphoreType.REGULAR((4 * L,)),
+        dma((2,)),
+        dma((2,)),
+        dma,
+        dma,
     ]
     return pl.pallas_call(
         functools.partial(fused_kernel, S, T, L),

time: 168 us -> 153 us (0.911); the launches traced: 167 us -> 150 us
  Pallas kernels: 165 us -> 148 us
    pallas_call x1, Pallas kernels: 165 us -> 148 us  [fused(): pl.pallas_call(functools.partial(fused_kernel, S, T, L), out_shape=jax.Sh...]
where the time goes in v2:
time: 153 us; the launch traced here: 150 us
  Pallas kernels  148 us (97%)
  local copies, waits for them, and re-layouts  1.87 us (1%)
    pallas_call x1, Pallas kernels, fused(): pl.pallas_call(functools.partial(fused_kernel, S, T, L), out_shape=jax.Sh...  148 us

profile of v2, /device:TPU:5, one launch (start us, length us, event | category | flops | bytes accessed | tf_op | source)
XLA Modules:
  0.0 150.3 jit_solution(2952674336537859981)
XLA Ops:
  0.0 148.4 %shard_map.82 = bf16[512,512]{1,0:T(8,128)(2,1)} custom-call(bf16[512,512]{1,0:T(8,128)(2,1)} %stream_ref.1, s32[4,128]{1,0:T(4,128)} %bitcast.3, f32[2,2048]{1,0:T(2,128)} %gain_ref.1, bf16[2,256,512]{2,1,0:T(8,128)(2,1)} %gate_ref.1, bf16[2,256,512]{2,1,0:T(8,128)(2,1)} %input_ref.1, bf16[2,256,512]{2,1,0:T(8,128)(2,1)} %value_ref.1, ...), custom_call_target="tpu_custom_call" | custom-call | tf_op jit(solution)/shard_map/pallas_call | solution.py:615
  148.4 1.9 %copy.10 = bf16[512,512]{1,0:T(8,128)(2,1)} copy(bf16[512,512]{1,0:T(8,128)(2,1)} %shard_map.82) | data formatting | bytes 1048576

commit v3 on v2

--- a/solution.py
+++ b/solution.py
@@ -354,47 +354,60 @@
     def zs_copy(layer, i):
         return remote(zsrc.at[layer, i], zrcv.at[layer, i], z_send.at[layer, i], z_recv.at[layer, i], (mate, t))
 
-    def sweep(use):
-        def step(e, carry):
-            use(e % per, e // per)
-            return carry
-
-        lax.fori_loop(0, 2 * per, step, 0)
+    first, second = y, 1 - y
 
     def partial(layer, dx, dc, i, tb):
         shard = owner_of(dx, dc) * per + i
         return jnp.dot(gated[lax.rem(theirs + tb, 2)], wout[layer, shard], preferred_element_type=f32)
 
-    def hand_over(layer, dx):
-        def use(i, tb):
-            dsrc[layer, dx, i, tb] = partial(layer, dx, 1, i, tb).astype(bf)
-            d_copy(layer, dx, i, tb).start()
-
-        sweep(use)
-
-    def send_across(layer):
-        def use(i, tb):
-            part = partial(layer, 1, 0, i, tb)
-            d_copy(layer, 1, i, tb).wait_recv()
-            xsrc[layer, i, tb] = (part + drcv[layer, 1, i, tb].astype(f32)).astype(bf)
-            xs_copy(layer, i, tb).start()
-
-        sweep(use)
-
-    def hold(layer):
-        def use(i, tb):
-            part = partial(layer, 0, 0, i, tb)
-            d_copy(layer, 0, i, tb).wait_recv()
-            acc[i, tb] = part + drcv[layer, 0, i, tb].astype(f32)
-
-        sweep(use)
+    def each_block(use):
+        def step(tb, carry):
+            use(tb)
+            return carry
+
+        lax.fori_loop(0, 2, step, 0)
 
     def joined(layer, dx, i, tb):
         part = partial(layer, dx, 0, i, tb)
         d_copy(layer, dx, i, tb).wait_recv()
         return part + drcv[layer, dx, i, tb].astype(f32)
 
-    tail = per - 1
+    def hand_over(layer, dx, i):
+        def use(tb):
+            dsrc[layer, dx, i, tb] = partial(layer, dx, 1, i, tb).astype(bf)
+            d_copy(layer, dx, i, tb).start()
+
+        each_block(use)
+
+    def send_across(layer, i, tb):
+        xsrc[layer, i, tb] = joined(layer, 1, i, tb).astype(bf)
+        xs_copy(layer, i, tb).start()
+
+    def hold(layer, i):
+        def use(tb):
+            acc[i, tb] = joined(layer, 0, i, tb)
+
+        each_block(use)
+
+    def to_mate(layer, i):
+        xs_copy(layer, i, 0).wait_recv()
+        zsrc[layer, i] = (acc[i, 0] + xrcv[layer, i, 0].astype(f32)).astype(bf)
+        go(lambda: zs_copy(layer, i))
+
+    def settle(layer, i, total):
+        fresh = (xfull[layer, zl, t, i].astype(f32) + total).astype(bf)
+        if layer + 1 < L:
+            xfull[layer + 1, zl, t, i] = fresh
+        else:
+            for which in range(per):
+                @pl.when(i == which)
+                def _():
+                    result_ref[:, which * ow:(which + 1) * ow] = fresh
+
+    def finish(layer, i):
+        xs_copy(layer, i, 1).wait_recv()
+        zs_copy(layer, i).wait_recv()
+        settle(layer, i, acc[i, 1] + xrcv[layer, i, 1].astype(f32) + zrcv[layer, i].astype(f32))
 
     def zq_copy(dx):
         return remote(zqsrc.at[dx], zqrcv.at[dx], zq_send.at[dx], zq_recv.at[dx], (mate, t))
@@ -402,51 +415,26 @@
     def xq_copy():
         return remote(xqsrc, xqrcv, xq_send, xq_recv, (s, across))
 
-    def to_mate_first(layer, dx):
-        zqsrc[dx] = joined(layer, dx, tail, 0).astype(bf)
+    def cross_first(layer, i, dx):
+        zqsrc[dx] = joined(layer, dx, i, 0).astype(bf)
         go(lambda: zq_copy(dx))
 
-    def send_both(layer):
-        to_mate_first(layer, 1)
-        for tb in range(2):
-            for i in range(tail):
-                xsrc[layer, i, tb] = joined(layer, 1, i, tb).astype(bf)
-                go(lambda i=i, tb=tb: xs_copy(layer, i, tb))
-        accq[...] = joined(layer, 1, tail, 1)
-
-    def hold_both(layer):
-        to_mate_first(layer, 0)
-        for tb in range(2):
-            for i in range(tail):
-                acc[i, tb] = joined(layer, 0, i, tb)
-        acc[tail, 1] = joined(layer, 0, tail, 1)
+    def cross_hold(layer, i, dx):
+        held = joined(layer, dx, i, 1)
+        if dx == 1:
+            accq[...] = held
+        else:
+            acc[i, 1] = held
 
     def cross_sum():
         zq_copy(1).wait_recv()
         xqsrc[...] = (accq[...] + zqrcv[1].astype(f32)).astype(bf)
         go(xq_copy)
 
-    def finish_crossed(layer):
+    def finish_crossed(layer, i):
         zq_copy(0).wait_recv()
         xq_copy().wait_recv()
-        total = acc[tail, 1] + zqrcv[0].astype(f32) + xqrcv[...].astype(f32)
-        fresh = (xfull[layer, zl, t, tail].astype(f32) + total).astype(bf)
-        result_ref[:, tail * ow:(tail + 1) * ow] = fresh
-
-    def to_mate(layer, i):
-        xs_copy(layer, i, 0).wait_recv()
-        zsrc[layer, i] = (acc[i, 0] + xrcv[layer, i, 0].astype(f32)).astype(bf)
-        go(lambda: zs_copy(layer, i))
-
-    def finish(layer, i):
-        xs_copy(layer, i, 1).wait_recv()
-        zs_copy(layer, i).wait_recv()
-        total = acc[i, 1] + xrcv[layer, i, 1].astype(f32) + zrcv[layer, i].astype(f32)
-        fresh = (xfull[layer, zl, t, i].astype(f32) + total).astype(bf)
-        if layer + 1 < L:
-            xfull[layer + 1, zl, t, i] = fresh
-        else:
-            result_ref[:, i * ow:(i + 1) * ow] = fresh
+        settle(layer, i, acc[i, 1] + zqrcv[0].astype(f32) + xqrcv[...].astype(f32))
 
     for layer in range(L):
         base = 4 * layer
@@ -466,14 +454,13 @@
             begin(3)
         else:
             pump(base + 2)
-            ag_from_z(layer, 0)
-            for i in range(per):
-                ag_from_x(layer, zl, i)
+            ag_from_z(layer, first)
+            ag_from_x(layer, zl, first)
+            ag_from_x(layer, zl, second)
         ag_from_core(layer, zl)
         norm(layer, zl)
         if layer > 0:
-            for i in range(1, per):
-                ag_from_z(layer, i)
+            ag_from_z(layer, second)
         need(base)
         project(layer, 0, zl)
         if layer == 0:
@@ -485,15 +472,17 @@
             pump(2, Z - 1, Z)
         else:
             pump(base + 3)
-        for i in range(per):
-            ag_from_x(layer, theirs, i)
+        ag_from_x(layer, theirs, first)
+        ag_from_x(layer, theirs, second)
         ag_from_core(layer, theirs)
         norm(layer, theirs)
         project(layer, 0, theirs)
+        if layer == 0:
+            pump(3, 1, 2)
         project(layer, 1, theirs)
         send_edges(layer, theirs)
         if layer == 0:
-            pump(3)
+            pump(3, 2, Z)
         if not last:
             begin(base + 4)
         need(base + 2)
@@ -503,36 +492,46 @@
             meet(base + 3)
             begin(base + 5)
         convolve(layer)
-        need(base + 3)
-        if not last:
+        if last:
+            need(base + 3)
+            hand_over(layer, 1, second)
+            hand_over(layer, 1, first)
+            cross_first(layer, second, 1)
+            send_across(layer, first, 0)
+            send_across(layer, first, 1)
+            cross_hold(layer, second, 1)
+            hand_over(layer, 0, second)
+            hand_over(layer, 0, first)
+            cross_first(layer, second, 0)
+            hold(layer, first)
+            cross_hold(layer, second, 0)
+            to_mate(layer, first)
+            cross_sum()
+            finish(layer, first)
+            finish_crossed(layer, second)
+        else:
+            hand_over(layer, 1, first)
+            send_across(layer, first, 0)
+            hand_over(layer, 0, first)
+            hold(layer, first)
+            need(base + 3)
             begin(base + 6)
+            hand_over(layer, 1, second)
+            send_across(layer, second, 0)
+            send_across(layer, first, 1)
+            send_across(layer, second, 1)
             for u in range(base + 4, base + 8):
                 own_y(u)
-        hand_over(layer, 1)
-        if last:
-            send_both(layer)
-        else:
-            send_across(layer)
-        hand_over(layer, 0)
-        if last:
-            hold_both(layer)
-        else:
-            hold(layer)
-        if not last:
+            hand_over(layer, 0, second)
+            hold(layer, second)
+            to_mate(layer, first)
+            to_mate(layer, second)
             pump(base + 4)
-        for i in range(per - 1 if last else per):
-            to_mate(layer, i)
-        if last:
-            cross_sum()
-        else:
+            finish(layer, first)
+            ag_own(layer + 1, first)
             pump(base + 5)
-        for i in range(per - 1 if last else per):
-            finish(layer, i)
-            if not last:
-                ag_own(layer + 1, i)
-        if last:
-            finish_crossed(layer)
-        else:
+            finish(layer, second)
+            ag_own(layer + 1, second)
             begin(base + 7)
 
     for copy_of, cond in pending:
@@ -541,13 +540,16 @@
         else:
             pl.when(cond)(lambda copy_of=copy_of: copy_of().wait_send())
     for layer in range(L):
-        def drain(i, tb):
-            for dx in range(2):
-                d_copy(layer, dx, i, tb).wait_send()
-            if layer + 1 < L:
-                xs_copy(layer, i, tb).wait_send()
-
-        sweep(drain)
+        for i in range(per):
+            def drain(tb):
+                for dx in range(2):
+                    d_copy(layer, dx, i, tb).wait_send()
+
+                @pl.when(jnp.logical_or(layer + 1 < L, i == first))
+                def _():
+                    xs_copy(layer, i, tb).wait_send()
+
+            each_block(drain)
 
 
 def fused(S, T, stream, doc_ids, norm_gain, gate_proj, input_gate, value_proj, taps, out_proj):
@@ -628,7 +630,7 @@
 
     def body(*arrays):
         (rows, width), cols, out_width = arrays[0].shape, arrays[3].shape[2], arrays[7].shape[2]
-        aligned = out_width % 128 == 0 and cols % 256 == 0 and rows % 128 == 0 and width % out_width == 0
+        aligned = out_width % 128 == 0 and cols % 256 == 0 and rows % 128 == 0 and width == 2 * out_width
         if aligned and sp % 4 == 0 and tp == 4:
             return fused(sp, tp, *arrays)
         return per_device(*arrays)

time: 153 us -> 151 us (0.987)
  no operation moved by 1% of the time
where the time goes in v3:
time: 151 us; the launch traced here: 150 us
  Pallas kernels  148 us (98%)
  local copies, waits for them, and re-layouts  1.87 us (1%)
    pallas_call x1, Pallas kernels, fused(): pl.pallas_call(functools.partial(fused_kernel, S, T, L), out_shape=jax.Sh...  148 us

profile of v3, /device:TPU:5, one launch (start us, length us, event | category | flops | bytes accessed | tf_op | source)
XLA Modules:
  0.0 149.6 jit_solution(14689517876283227893)
XLA Ops:
  0.0 147.7 %shard_map.82 = bf16[512,512]{1,0:T(8,128)(2,1)} custom-call(bf16[512,512]{1,0:T(8,128)(2,1)} %stream_ref.1, s32[4,128]{1,0:T(4,128)} %bitcast.3, f32[2,2048]{1,0:T(2,128)} %gain_ref.1, bf16[2,256,512]{2,1,0:T(8,128)(2,1)} %gate_ref.1, bf16[2,256,512]{2,1,0:T(8,128)(2,1)} %input_ref.1, bf16[2,256,512]{2,1,0:T(8,128)(2,1)} %value_ref.1, ...), custom_call_target="tpu_custom_call" | custom-call | tf_op jit(solution)/shard_map/pallas_call | solution.py:617
  147.7 1.9 %copy.10 = bf16[512,512]{1,0:T(8,128)(2,1)} copy(bf16[512,512]{1,0:T(8,128)(2,1)} %shard_map.82) | data formatting | bytes 1048576

commit v4 on v3

--- a/solution.py
+++ b/solution.py
@@ -471,6 +471,8 @@
         if layer == 0:
             pump(2, Z - 1, Z)
         else:
+            need(base + 2)
+            project(layer, 2, zl)
             pump(base + 3)
         ag_from_x(layer, theirs, first)
         ag_from_x(layer, theirs, second)
@@ -485,8 +487,9 @@
             pump(3, 2, Z)
         if not last:
             begin(base + 4)
-        need(base + 2)
-        project(layer, 2, zl)
+        if layer == 0:
+            need(base + 2)
+            project(layer, 2, zl)
         project(layer, 2, theirs)
         if not last:
             meet(base + 3)

time: 151 us -> 151 us (level)
  no operation moved by 1% of the time
where the time goes in v4:
time: 151 us; the launch traced here: 150 us
  Pallas kernels  148 us (98%)
  local copies, waits for them, and re-layouts  1.87 us (1%)
    pallas_call x1, Pallas kernels, fused(): pl.pallas_call(functools.partial(fused_kernel, S, T, L), out_shape=jax.Sh...  148 us

profile of v4, /device:TPU:5, one launch (start us, length us, event | category | flops | bytes accessed | tf_op | source)
XLA Modules:
  0.0 149.6 jit_solution(15892501526579827938)
XLA Ops:
  0.0 147.7 %shard_map.82 = bf16[512,512]{1,0:T(8,128)(2,1)} custom-call(bf16[512,512]{1,0:T(8,128)(2,1)} %stream_ref.1, s32[4,128]{1,0:T(4,128)} %bitcast.3, f32[2,2048]{1,0:T(2,128)} %gain_ref.1, bf16[2,256,512]{2,1,0:T(8,128)(2,1)} %gate_ref.1, bf16[2,256,512]{2,1,0:T(8,128)(2,1)} %input_ref.1, bf16[2,256,512]{2,1,0:T(8,128)(2,1)} %value_ref.1, ...), custom_call_target="tpu_custom_call" | custom-call | tf_op jit(solution)/shard_map/pallas_call | solution.py:620
  147.7 1.9 %copy.10 = bf16[512,512]{1,0:T(8,128)(2,1)} copy(bf16[512,512]{1,0:T(8,128)(2,1)} %shard_map.82) | data formatting | bytes 1048576
